TPU v7x, 32 devices: a whole 2x2x4 slice. The times are simulated.
32 devices in a mesh: ep: 16 (over z, y, x), tp: 2 (over core).
Axes of the slice: x: 2, y: 2, z: 4, core: 2. Of those that a mesh axis runs over, the one named last changes fastest.
Arguments:
- tokens: bfloat16 [256, 2048], P('ep'), may hold values from -6 to 6
- lengths: int32 [256], P('ep'), may hold values from 1024 to 8191
- prior_state: float32 [256, 16, 64, 64], P('ep', 'tp'), may hold values from -2 to 2
- mix_gain: float32 [2048], replicated, may hold values from 0.1 to 1.9
- post_gain: float32 [2048], replicated, may hold values from 0.1 to 1.9
- ffn_gain: float32 [2048], replicated, may hold values from 0.1 to 1.9
- out_gain: float32 [2048], replicated, may hold values from 0.1 to 1.9
- query_weight: bfloat16 [2048, 1024], P('ep', 'tp'), may hold values from -0.125 to 0.125
- key_weight: bfloat16 [2048, 1024], P('ep', 'tp'), may hold values from -0.125 to 0.125
- value_weight: bfloat16 [2048, 1024], P('ep', 'tp'), may hold values from -0.125 to 0.125
- gate_weight: bfloat16 [2048, 1024], P('ep', 'tp'), may hold values from -0.125 to 0.125
- out_weight: bfloat16 [1024, 2048], P('tp', 'ep'), may hold values from -0.1875 to 0.1875
- routes: int32 [256, 6], P('ep'), may hold values from 0 to 15, all different within a row; in each aligned block of 16 rows (0 to 15, 16 to 31, ...) at most 8 rows name the same one
- route_gates: float32 [256, 6], P('ep'), may hold values from 0.1 to 0.9
- expert_gate: bfloat16 [16, 2048, 512], P('ep', None, 'tp'), may hold values from -0.125 to 0.125
- expert_up: bfloat16 [16, 2048, 512], P('ep', None, 'tp'), may hold values from -0.125 to 0.125
- expert_down: bfloat16 [16, 512, 2048], P('ep', 'tp'), may hold values from -0.25 to 0.25
- shared_gate: bfloat16 [2048, 512], P(None, 'tp'), may hold values from -0.125 to 0.125
- shared_up: bfloat16 [2048, 512], P(None, 'tp'), may hold values from -0.125 to 0.125
- shared_down: bfloat16 [512, 2048], P('tp'), may hold values from -0.25 to 0.25
Outputs:
- result: bfloat16 [256, 2048], P('ep')
- new_state: float32 [256, 16, 64, 64], P('ep', 'tp')
Inputs may be any that keep to these rules, and one draw needn't show every extreme that they name: `routes`: each row names 6 different experts. In the rows of one device (aligned blocks of 16 rows) no expert is named more than 8 times, and in every draw some expert is named exactly 8 times in some block.
All inputs are finite; a program needn't handle non-finite values.
Results may differ from a plain program's by a relative error of at most 0.02.
Values may be sent and summed in bfloat16 or wider, within the bound.
A program may use at most 128 MiB of HBM per device.

v0:
```python
import jax
import jax.numpy as jnp
from jax import lax
from jax.sharding import PartitionSpec as P

HEAD = 64
HEADS = 16
EPS = 1e-06
THETA = 10000.0


def rounded(values):
    return lax.optimization_barrier(values.astype(jnp.bfloat16)).astype(jnp.float32)


def scaled_rows(values, gain_row):
    widened = values.astype(jnp.float32)
    return widened * lax.rsqrt(jnp.mean(widened * widened, axis=-1, keepdims=True) + EPS) * gain_row


def rotate(vectors, lengths):
    half_dim = vectors.shape[-1] // 2
    frequency = THETA ** (-jnp.arange(half_dim, dtype=jnp.float32) / half_dim)
    angles = lengths.astype(jnp.float32)[:, None] * frequency[None, :]
    cosine = jnp.cos(angles)[:, None, :]
    sine_part = jnp.sin(angles)[:, None, :]
    leading = vectors[..., :half_dim]
    trailing = vectors[..., half_dim:]
    return jnp.concatenate(
        [leading * cosine - trailing * sine_part, trailing * cosine + leading * sine_part], axis=-1
    )


def decay_table(head_count):
    head_order = jnp.arange(head_count, dtype=jnp.float32)
    return 1.0 - jnp.exp2(-5.0 - 7.0 * head_order / (head_count - 1))


def retain(queries, keys_new, values, out_gate, prior_state, lengths, decays):
    seq_count = queries.shape[0]
    head_count = decays.shape[0]
    layout = (seq_count, head_count, HEAD)
    rot_query = rotate(queries.astype(jnp.float32).reshape(layout), lengths)
    rot_key = rotate(keys_new.astype(jnp.float32).reshape(layout), lengths) * HEAD ** (-0.5)
    wide_values = values.astype(jnp.float32).reshape(layout)
    from_state = jnp.einsum(
        "shd,shde->she", rot_query, prior_state, precision=lax.Precision.HIGHEST
    )
    self_term = jnp.sum(rot_query * rot_key, axis=-1, keepdims=True)
    read_out = decays[None, :, None] * from_state + self_term * wide_values
    new_state = (
        decays[None, :, None, None] * prior_state
        + rot_key[..., :, None] * wide_values[..., None, :]
    )
    normed = read_out * lax.rsqrt(jnp.mean(read_out * read_out, axis=-1, keepdims=True) + EPS)
    gated_rows = normed.reshape(seq_count, head_count * HEAD) * jax.nn.silu(
        out_gate.astype(jnp.float32)
    )
    return (gated_rows.astype(jnp.bfloat16), new_state)


def on_device(
    tokens,
    lengths,
    prior_state,
    mix_gain,
    post_gain,
    ffn_gain,
    out_gain,
    query_weight,
    key_weight,
    value_weight,
    gate_weight,
    out_weight,
    routes,
    route_gates,
    expert_gate,
    expert_up,
    expert_down,
    shared_gate,
    shared_up,
    shared_down,
):
    seq_here = tokens.shape[0]
    model_width = tokens.shape[1]
    local_cols = query_weight.shape[1]
    normed = scaled_rows(tokens, mix_gain).astype(jnp.bfloat16)
    features = lax.all_to_all(normed, "ep", split_axis=1, concat_axis=0, tiled=True)
    joined = jnp.concatenate((query_weight, key_weight, value_weight, gate_weight), axis=1)
    summed = lax.psum_scatter(
        jnp.dot(features, joined, preferred_element_type=jnp.float32),
        "ep",
        scatter_dimension=0,
        tiled=True,
    )
    projected = tuple((summed[:, role * local_cols : (role + 1) * local_cols] for role in range(4)))
    queries, keys_new, values, out_gate = tuple(
        (member.astype(jnp.bfloat16) for member in projected)
    )
    heads_here = local_cols // HEAD
    decays = lax.dynamic_slice_in_dim(
        decay_table(HEADS), lax.axis_index("tp") * heads_here, heads_here, 0
    )
    retained, new_state = retain(queries, keys_new, values, out_gate, prior_state, lengths, decays)
    column_part = jnp.dot(
        lax.all_gather(retained, "ep", axis=0, tiled=True),
        out_weight,
        preferred_element_type=jnp.float32,
    ).astype(jnp.bfloat16)
    partial_mix = lax.all_to_all(column_part, "ep", split_axis=0, concat_axis=1, tiled=True).astype(
        jnp.float32
    )
    mixed_sum = rounded(
        lax.psum(rounded(partial_mix).astype(jnp.bfloat16), "tp").astype(jnp.float32)
    )
    middle = rounded(tokens.astype(jnp.float32) + scaled_rows(mixed_sum, post_gain))
    moe_in = scaled_rows(middle, ffn_gain).astype(jnp.bfloat16)
    experts_all = lax.axis_size("ep")
    topk_here = routes.shape[1]
    capacity = seq_here * topk_here // experts_all + 2
    slot_count = experts_all * capacity
    flat_routes = routes.reshape(-1)
    onehot = (flat_routes[:, None] == jnp.arange(experts_all, dtype=jnp.int32)[None, :]).astype(
        jnp.int32
    )
    earlier = jnp.cumsum(onehot, axis=0) - onehot
    ranks = jnp.sum(earlier * onehot, axis=1)
    slot_ids = flat_routes * capacity + ranks
    placing = (jnp.arange(slot_count, dtype=jnp.int32)[:, None] == slot_ids[None, :]).reshape(
        slot_count, seq_here, topk_here
    )
    dispatch_rows = jnp.any(placing, axis=2).astype(jnp.bfloat16)
    combine = jnp.sum(
        jnp.where(placing, route_gates[None, :, :], jnp.zeros((), jnp.float32)), axis=2
    ).T
    outgoing = jnp.dot(dispatch_rows, moe_in, preferred_element_type=jnp.float32).astype(
        jnp.bfloat16
    )
    outgoing = outgoing.reshape(experts_all, capacity, model_width)
    gate_local = expert_gate[0]
    up_local = expert_up[0]
    down_local = expert_down[0]
    arrived = lax.all_to_all(outgoing, "ep", split_axis=0, concat_axis=0, tiled=True)
    sources = arrived.shape[0]
    held_slots = arrived.shape[1]
    flat_in = arrived.reshape(sources * held_slots, model_width)
    hidden = (
        jax.nn.silu(jnp.dot(flat_in, gate_local, preferred_element_type=jnp.float32))
        * jnp.dot(flat_in, up_local, preferred_element_type=jnp.float32)
    ).astype(jnp.bfloat16)
    partial_out = rounded(jnp.dot(hidden, down_local, preferred_element_type=jnp.float32))
    expert_sum = lax.psum(partial_out.astype(jnp.bfloat16), "tp")
    returned = lax.all_to_all(
        expert_sum.reshape(sources, held_slots, -1), "ep", split_axis=0, concat_axis=0, tiled=True
    )
    back_rows = returned.reshape(slot_count, -1).astype(jnp.float32)
    routed = jnp.dot(combine, back_rows, precision=lax.Precision.HIGHEST)
    shared_hidden = (
        jax.nn.silu(jnp.dot(moe_in, shared_gate, preferred_element_type=jnp.float32))
        * jnp.dot(moe_in, shared_up, preferred_element_type=jnp.float32)
    ).astype(jnp.bfloat16)
    shared_part = rounded(jnp.dot(shared_hidden, shared_down, preferred_element_type=jnp.float32))
    shared_out = lax.psum(shared_part.astype(jnp.bfloat16), "tp")
    mixture = shared_out.astype(jnp.float32) + routed
    result = (middle + scaled_rows(mixture, out_gain)).astype(jnp.bfloat16)
    return (result, new_state)


def solution(mesh):
    return jax.shard_map(
        on_device,
        mesh=mesh,
        in_specs=(
            P("ep", None),
            P("ep"),
            P("ep", "tp", None, None),
            P(),
            P(),
            P(),
            P(),
            P("ep", "tp"),
            P("ep", "tp"),
            P("ep", "tp"),
            P("ep", "tp"),
            P("tp", "ep"),
            P("ep", None),
            P("ep", None),
            P("ep", None, "tp"),
            P("ep", None, "tp"),
            P("ep", "tp", None),
            P(None, "tp"),
            P(None, "tp"),
            P("tp", None),
        ),
        out_specs=(P("ep", None), P("ep", "tp", None, None)),
        check_vma=False,
    )
```

profile of v0, /device:TPU:0, one launch (start us, length us, event | category | flops | bytes accessed | tf_op | source)
XLA Modules:
  0.0 254.3 jit_solution(6704595756294250518)
XLA Ops:
  7.2 0.0 copy-start
  7.2 0.0 copy-start.10
  7.2 0.0 reduce-scatter.2.cloned.1.call-start
  7.2 1.0 fusion.25
  8.3 0.9 copy_bitcast_fusion.1
  9.2 15.7 %all_to_all.48 = bf16[16,16,128]{2,0,1:T(8,128)(2,1)S(1)} all-to-all(bf16[16,16,128]{2,0,1:T(8,128)(2,1)S(1)} %copy_bitcast_fusion.1), channel_id=1, replica_groups=mesh['ep'=16,'tp'=2] {'ep'}, dimensions={1} | all-to-all | bytes 131072 | tf_op jit(solution)/shard_map/all_to_all | solution.py:88
  24.9 2.8 %fusion.11 = f32[256,2048]{1,0:T(8,128)} fusion(bf16[256,128]{1,0:T(8,128)(2,1)S(1)} %bitcast.57, bf16[128,512]{1,0:T(8,128)(2,1)} %param.30, bf16[128,512]{1,0:T(8,128)(2,1)} %param.29, bf16[128,512]{1,0:T(8,128)(2,1)} %param.28, bf16[128,512]{1,0:T(8,128)(2,1)} %param.27), kind=kOutput, calls=%fused_computation.18 | convolution fusion | flops 136314880 | bytes 2686976 | tf_op jit(solution)/shard_map/dot_general | solution.py:91
  27.7 0.0 reduce-scatter.2.cloned.1.call-update
  27.8 0.0 copy-start.2
  27.8 0.0 copy-start.7
  27.8 0.0 copy-start.4
  27.8 0.1 copy.38
  27.9 0.1 eq.30
  28.0 0.1 fusion.40
  28.1 0.1 reduce_window_sum.11
  28.2 0.2 select_reduce_fusion.1
  28.4 0.1 reduce_sum.80
  28.5 0.1 copy.39
  28.6 0.1 dynamic_slice.3
  28.7 0.1 multiply_cosine_fusion
  28.8 77.1 %reduce-scatter.2.cloned.1.call-done = f32[16,2048]{1,0:T(8,128)} async-done(((f32[256,2048]{1,0:T(8,128)}), f32[16,2048]{1,0:T(8,128)}) %reduce-scatter.2.cloned.1.call-update) | async-done | bytes 131088 | tf_op jit(solution)/shard_map/reduce_scatter | solution.py:90
  105.9 0.9 convert.9
  106.8 0.1 reshape.191
  106.9 0.1 reshape.193
  107.0 0.1 reshape.189
  107.1 0.1 multiply_subtract_fusion
  107.2 0.1 pad_maximum_fusion
  107.3 5.3 %fusion.62 = f32[16,8,1,64]{3,2,1,0:T(1,128)S(1)} fusion(f32[16,8,64,1]{2,3,1,0:T(1,128)S(1)} %bitcast.55, f32[16,8,64,64]{3,2,1,0:T(8,128)} %param.22), kind=kOutput, calls=%fused_computation.103 | convolution fusion | flops 6291456 | bytes 2162688 | tf_op jit(solution)/shard_map/shd,shde->she/dot_general | solution.py:46
  112.6 0.2 multiply_reduce_fusion.1
  112.8 0.1 broadcast_multiply_fusion
  112.9 0.0 copy-start.1
  112.9 0.1 reshape.183
  113.0 38.2 %all_gather.3 = bf16[256,512]{1,0:T(8,128)(2,1)S(1)} all-gather(bf16[16,512]{1,0:T(8,128)(2,1)S(1)} %fusion.46), channel_id=1, replica_groups=mesh['ep'=16,'tp'=2] {'ep'}, dimensions={0}, use_global_device_ids=true | all-gather | bytes 278528 | tf_op jit(solution)/shard_map/all_gather | solution.py:106
  151.2 0.0 copy-done.3
  151.2 0.8 convolution_convert_fusion.3
  152.1 3.5 %all-to-all-start.1 = ((bf16[16,16,128]{2,1,0:T(8,128)(2,1)}), bf16[16,16,128]{2,1,0:T(8,128)(2,1)S(1)}, u32[]{:S(2)}, u32[]{:S(2)}) async-start(bf16[16,16,128]{2,1,0:T(8,128)(2,1)} %bitcast.6), calls=%async_computation.2 | async-start | bytes 131072 | tf_op jit(solution)/shard_map/all_to_all | solution.py:110
  155.6 0.0 all-reduce.4.cloned.1.call-start
  155.6 7.4 %all-to-all-done.1 = bf16[16,16,128]{2,1,0:T(8,128)(2,1)S(1)} async-done(((bf16[16,16,128]{2,1,0:T(8,128)(2,1)}), bf16[16,16,128]{2,1,0:T(8,128)(2,1)S(1)}, u32[]{:S(2)}, u32[]{:S(2)}) %all-to-all-start.1) | async-done | bytes 65568 | tf_op jit(solution)/shard_map/all_to_all | solution.py:110
  163.1 0.6 copy_bitcast_fusion
  163.7 0.0 all-reduce.4.cloned.1.call-update
  163.7 0.1 fusion.41
  163.8 14.5 %all-reduce.4.cloned.1.call-done = bf16[16,2048]{1,0:T(8,128)(2,1)} async-done(((bf16[16,2048]{1,0:T(8,128)(2,1)}), bf16[16,2048]{1,0:T(8,128)(2,1)}) %all-reduce.4.cloned.1.call-update) | async-done | bytes 65552 | tf_op jit(solution)/shard_map/psum | solution.py:114
  178.3 1.0 fusion.23
  179.3 0.0 copy-done.2
  179.3 0.9 fusion.28
  180.2 0.1 fusion.29
  180.4 1.1 fusion.1
  181.5 6.8 %all-to-all-start.2 = ((bf16[16,8,2048]{2,1,0:T(8,128)(2,1)}), bf16[16,8,2048]{2,1,0:T(8,128)(2,1)S(1)}, u32[]{:S(2)}, u32[]{:S(2)}) async-start(bf16[16,8,2048]{2,1,0:T(8,128)(2,1)} %fusion.1), calls=%async_computation.3 | async-start | bytes 1048576 | tf_op jit(solution)/shard_map/all_to_all | solution.py:143
  188.4 0.0 all-reduce.6.cloned.1.call-start
  188.4 1.5 fusion.60
  189.9 3.0 %convolution_convert_fusion.2 = bf16[16,2048]{1,0:T(8,128)(2,1)} fusion(bf16[256,2048]{1,0:T(8,128)(2,1)} %param.39, bf16[2048,256]{1,0:T(8,128)(2,1)} %param.38, f32[16,256]{1,0:T(8,128)S(1)} %fusion.60, bf16[16,2048]{1,0:T(8,128)(2,1)S(1)} %fusion.28, f32[2048]{0:T(1024)S(1)} %copy-done.4, f32[16]{0:T(128)S(1)} %add_rsqrt_fusion.2), kind=kOutput, calls=%fused_computation.6 | convolution fusion | flops 33742848 | bytes 2252864 | tf_op jit(solution)/shard_map/dot_general | solution.py:162
  192.9 10.9 %all-to-all-done.2 = bf16[16,8,2048]{2,1,0:T(8,128)(2,1)S(1)} async-done(((bf16[16,8,2048]{2,1,0:T(8,128)(2,1)}), bf16[16,8,2048]{2,1,0:T(8,128)(2,1)S(1)}, u32[]{:S(2)}, u32[]{:S(2)}) %all-to-all-start.2) | async-done | bytes 524320 | tf_op jit(solution)/shard_map/all_to_all | solution.py:143
  203.8 1.5 fusion.9
  205.4 1.6 convolution_convert_fusion
  207.0 0.0 all-reduce.6.cloned.1.call-update
  207.0 17.3 %all-reduce.6.cloned.1.call-done = (bf16[16,8,2048]{2,1,0:T(8,128)(2,1)}, bf16[16,2048]{1,0:T(8,128)(2,1)}) async-done(((bf16[16,8,2048]{2,1,0:T(8,128)(2,1)}, bf16[16,2048]{1,0:T(8,128)(2,1)}), (bf16[16,8,2048]{2,1,0:T(8,128)(2,1)}, bf16[16,2048]{1,0:T(8,128)(2,1)})) %all-reduce.6.cloned.1.call-update) | async-done | bytes 589840 | tf_op jit(solution)/shard_map/psum | solution.py:152
  224.3 6.8 %all-to-all-start.3 = ((bf16[16,8,2048]{2,1,0:T(8,128)(2,1)}), bf16[16,8,2048]{2,1,0:T(8,128)(2,1)S(1)}, u32[]{:S(2)}, u32[]{:S(2)}) async-start(bf16[16,8,2048]{2,1,0:T(8,128)(2,1)} %get-tuple-element.2), calls=%async_computation.4 | async-start | bytes 1048576 | tf_op jit(solution)/shard_map/all_to_all | solution.py:153
  231.1 0.1 select_reduce_fusion
  231.2 0.0 copy-start.5
  231.2 0.0 copy-start.8
  231.2 4.3 %multiply_add_fusion = f32[16,8,64,64]{3,2,1,0:T(8,128)} fusion(f32[16,8,64,64]{3,2,1,0:T(8,128)} %param.22, f32[16,8,64]{2,1,0:T(8,128)S(1)} %reshape.193, f32[16,8,64]{2,1,0:T(8,128)S(1)} %get-tuple-element.20, f32[8]{0:T(128)S(1)} %dynamic_slice.3), kind=kLoop, calls=%fused_computation.1 | loop fusion | flops 1572864 | bytes 4259872 | tf_op jit(solution)/shard_map/add | solution.py:52
  235.5 11.1 %all-to-all-done.3 = bf16[16,8,2048]{2,1,0:T(8,128)(2,1)S(1)} async-done(((bf16[16,8,2048]{2,1,0:T(8,128)(2,1)}), bf16[16,8,2048]{2,1,0:T(8,128)(2,1)S(1)}, u32[]{:S(2)}, u32[]{:S(2)}) %all-to-all-start.3) | async-done | bytes 524320 | tf_op jit(solution)/shard_map/all_to_all | solution.py:153
  246.6 0.4 multiply_reduce_fusion
  247.0 0.7 fusion.32
  (23 shorter events, 0.1 us)
Async XLA Ops:
  7.2 198.2 %copy-start = (bf16[1,256,2048]{2,1,0:T(8,128)(2,1)S(1)}, bf16[1,256,2048]{2,1,0:T(8,128)(2,1)}, u32[]{:S(2)}) copy-start(bf16[1,256,2048]{2,1,0:T(8,128)(2,1)} %param.36) | copy-start | bytes 3145732
  7.2 20.6 %copy-start.10 = (s32[16]{0:T(128)S(1)}, s32[16]{0:T(128)}, u32[]{:S(2)}) copy-start(s32[16]{0:T(128)} %param.21) | copy-start | bytes 196
  7.2 20.6 %copy-start.6 = (s32[16,6]{0,1:T(8,128)S(1)}, s32[16,6]{0,1:T(8,128)}, u32[]{:S(2)}) copy-start(s32[16,6]{0,1:T(8,128)} %param.32) | copy-start | bytes 1156
  7.2 98.7 %reduce-scatter.2.cloned.1.call-start = ((), (), s32[]{:S(2)}) async-start(), calls=%async_computation.5 | async-start | bytes 2228224 | tf_op jit(solution)/shard_map/reduce_scatter | solution.py:90
  27.7 123.5 %copy-start.3 = (bf16[512,128]{1,0:T(8,128)(2,1)S(1)}, bf16[512,128]{1,0:T(8,128)(2,1)}, u32[]{:S(2)}) copy-start(bf16[512,128]{1,0:T(8,128)(2,1)} %param.31) | copy-start | bytes 393220
  27.8 151.5 %copy-start.2 = (bf16[16,2048]{1,0:T(8,128)(2,1)S(1)}, bf16[16,2048]{1,0:T(8,128)(2,1)}, u32[]{:S(2)}) copy-start(bf16[16,2048]{1,0:T(8,128)(2,1)} %param.20) | copy-start | bytes 196612
  27.8 151.5 %copy-start.7 = (f32[2048]{0:T(1024)S(1)}, f32[2048]{0:T(1024)}, u32[]{:S(2)}) copy-start(f32[2048]{0:T(1024)} %param.24) | copy-start | bytes 24580
  27.8 152.6 %copy-start.4 = (f32[2048]{0:T(1024)S(1)}, f32[2048]{0:T(1024)}, u32[]{:S(2)}) copy-start(f32[2048]{0:T(1024)} %param.25) | copy-start | bytes 24580
  112.9 92.5 %copy-start.1 = (bf16[1,2048,256]{2,1,0:T(8,128)(2,1)S(1)}, bf16[1,2048,256]{2,1,0:T(8,128)(2,1)}, u32[]{:S(2)}) copy-start(bf16[1,2048,256]{2,1,0:T(8,128)(2,1)} %param.35) | copy-start | bytes 3145732
  152.1 11.0 %all-to-all-start.1 = ((bf16[16,16,128]{2,1,0:T(8,128)(2,1)}), bf16[16,16,128]{2,1,0:T(8,128)(2,1)S(1)}, u32[]{:S(2)}, u32[]{:S(2)}) async-start(bf16[16,16,128]{2,1,0:T(8,128)(2,1)} %bitcast.6), calls=%async_computation.2 | async-start | bytes 131072 | tf_op jit(solution)/shard_map/all_to_all | solution.py:110
  155.6 22.7 %all-reduce.4.cloned.1.call-start = ((), (), s32[]{:S(2)}) async-start(), calls=%async_computation.6 | async-start | bytes 131072 | tf_op jit(solution)/shard_map/psum | solution.py:114
  181.5 22.3 %all-to-all-start.2 = ((bf16[16,8,2048]{2,1,0:T(8,128)(2,1)}), bf16[16,8,2048]{2,1,0:T(8,128)(2,1)S(1)}, u32[]{:S(2)}, u32[]{:S(2)}) async-start(bf16[16,8,2048]{2,1,0:T(8,128)(2,1)} %fusion.1), calls=%async_computation.3 | async-start | bytes 1048576 | tf_op jit(solution)/shard_map/all_to_all | solution.py:143
  188.4 35.9 %all-reduce.6.cloned.1.call-start = ((), (), s32[]{:S(2)}) async-start(), calls=%async_computation.7 | async-start | bytes 1179648 | tf_op jit(solution)/shard_map/psum | solution.py:152
  189.9 41.2 %copy-start.9 = (f32[16,6]{0,1:T(8,128)S(1)}, f32[16,6]{0,1:T(8,128)}, u32[]{:S(2)}) copy-start(f32[16,6]{0,1:T(8,128)} %param.33) | copy-start | bytes 1156
  224.3 22.3 %all-to-all-start.3 = ((bf16[16,8,2048]{2,1,0:T(8,128)(2,1)}), bf16[16,8,2048]{2,1,0:T(8,128)(2,1)S(1)}, u32[]{:S(2)}, u32[]{:S(2)}) async-start(bf16[16,8,2048]{2,1,0:T(8,128)(2,1)} %get-tuple-element.2), calls=%async_computation.4 | async-start | bytes 1048576 | tf_op jit(solution)/shard_map/all_to_all | solution.py:153
  231.2 15.4 %copy-start.5 = (bf16[16,2048]{1,0:T(8,128)(2,1)S(1)}, bf16[16,2048]{1,0:T(8,128)(2,1)}, u32[]{:S(2)}) copy-start(bf16[16,2048]{1,0:T(8,128)(2,1)} %get-tuple-element.3) | copy-start | bytes 196612
  231.2 15.8 %copy-start.8 = (f32[2048]{0:T(1024)S(1)}, f32[2048]{0:T(1024)}, u32[]{:S(2)}) copy-start(f32[2048]{0:T(1024)} %param.26) | copy-start | bytes 24580
Sparse Core Ops, SparseCore 0:
  27.9 77.9 reduce-scatter.1
  163.9 14.3 all-reduce.3
  207.1 17.0 all-reduce.5
where the time goes:
time: 255 us; the launch traced here: 254 us
  waiting for transfers between devices  138 us (54%)
  blocking collectives  53.9 us (21%)
  matrix products  18.1 us (7%)
  starting transfers between devices  17.3 us (7%)
  between operations  14.1 us (6%)
  other arithmetic  11.2 us (4%)
    reduce_scatter x1, waiting for transfers between devices, on_device(): lax.psum_scatter(jnp.dot(features, joined, preferred_element_type=jnp.flo...  77.1 us
    all_gather x1, blocking collectives, on_device(): lax.all_gather(retained, 'ep', axis=0, tiled=True)  38.2 us
    psum x1, waiting for transfers between devices, on_device(): expert_sum = lax.psum(partial_out.astype(jnp.bfloat16), 'tp')  17.3 us
    all_to_all x1, blocking collectives, on_device(): lax.all_to_all(normed, 'ep', split_axis=1, concat_axis=0, tiled=True)  15.7 us
    psum x1, waiting for transfers between devices, on_device(): lax.psum(rounded(partial_mix).astype(jnp.bfloat16), 'tp')  14.5 us
    all_to_all x1, waiting for transfers between devices, on_device(): lax.all_to_all(expert_sum.reshape(sources, held_slots, -1), 'ep', split_a...  11.1 us
    all_to_all x1, waiting for transfers between devices, on_device(): lax.all_to_all(outgoing, 'ep', split_axis=0, concat_axis=0, tiled=True)  10.9 us
    all_to_all x1, waiting for transfers between devices, on_device(): lax.all_to_all(column_part, 'ep', split_axis=0, concat_axis=1, tiled=True)  7.44 us
  transfers between devices with their start and end apart: 6, of which 6 were waited for; matrix products, arithmetic and copies ran while one was open for 4% of the time, Pallas kernels for 0%

commit v1 on v0

--- a/solution.py
+++ b/solution.py
@@ -111,7 +111,9 @@
         jnp.float32
     )
     mixed_sum = rounded(
-        lax.psum(rounded(partial_mix).astype(jnp.bfloat16), "tp").astype(jnp.float32)
+        jnp.sum(jax.lax.all_gather(rounded(partial_mix).astype(jnp.bfloat16), "tp"), axis=0).astype(
+            jnp.float32
+        )
     )
     middle = rounded(tokens.astype(jnp.float32) + scaled_rows(mixed_sum, post_gain))
     moe_in = scaled_rows(middle, ffn_gain).astype(jnp.bfloat16)

time: 255 us -> 237 us (0.929)
  waiting for transfers between devices: 138 us -> 124 us
  starting transfers between devices: 17.3 us -> 14 us
    psum x1 -> x0, waiting for transfers between devices: 14.5 us -> none  [on_device(): lax.psum(rounded(partial_mix).astype(jnp.bfloat16), 'tp')]
    all_to_all x1, starting transfers between devices: 6.84 us -> 3.57 us  [on_device(): lax.all_to_all(outgoing, 'ep', split_axis=0, concat_axis=0, tiled=True)]
  transfers between devices with their start and end apart: 6 -> 5, of which waited for: 6 -> 5; matrix products, arithmetic and copies ran while one was open for 4% -> 4% of each run, Pallas kernels for 0% -> 0%
where the time goes in v1:
time: 237 us; the launch traced here: 236 us
  waiting for transfers between devices  124 us (52%)
  blocking collectives  55.3 us (23%)
  matrix products  18.1 us (8%)
  between operations  14.4 us (6%)
  starting transfers between devices  14 us (6%)
  other arithmetic  9.55 us (4%)
    reduce_scatter x1, waiting for transfers between devices, on_device(): lax.psum_scatter(jnp.dot(features, joined, preferred_element_type=jnp.flo...  77.4 us
    all_gather x1, blocking collectives, on_device(): lax.all_gather(retained, 'ep', axis=0, tiled=True)  37.8 us
    psum x1, waiting for transfers between devices, on_device(): expert_sum = lax.psum(partial_out.astype(jnp.bfloat16), 'tp')  17.4 us
    all_to_all x1, blocking collectives, on_device(): lax.all_to_all(normed, 'ep', split_axis=1, concat_axis=0, tiled=True)  15.7 us
    all_to_all x1, waiting for transfers between devices, on_device(): lax.all_to_all(expert_sum.reshape(sources, held_slots, -1), 'ep', split_a...  11.1 us
    all_to_all x1, waiting for transfers between devices, on_device(): lax.all_to_all(outgoing, 'ep', split_axis=0, concat_axis=0, tiled=True)  10.9 us
    all_to_all x1, waiting for transfers between devices, on_device(): lax.all_to_all(column_part, 'ep', split_axis=0, concat_axis=1, tiled=True)  7.4 us
    all_to_all x1, starting transfers between devices, on_device(): lax.all_to_all(expert_sum.reshape(sources, held_slots, -1), 'ep', split_a...  6.84 us
  transfers between devices with their start and end apart: 5, of which 5 were waited for; matrix products, arithmetic and copies ran while one was open for 4% of the time, Pallas kernels for 0%

profile of v1, /device:TPU:0, one launch (start us, length us, event | category | flops | bytes accessed | tf_op | source)
XLA Modules:
  0.0 236.3 jit_solution(9570223004432646994)
XLA Ops:
  7.2 0.0 copy-start
  7.2 0.0 copy-start.10
  7.2 0.0 copy-start.6
  7.2 0.0 reduce-scatter.2.cloned.1.call-start
  7.2 1.0 fusion.25
  8.3 0.9 copy_bitcast_fusion.1
  9.2 15.7 %all_to_all.48 = bf16[16,16,128]{2,0,1:T(8,128)(2,1)S(1)} all-to-all(bf16[16,16,128]{2,0,1:T(8,128)(2,1)S(1)} %copy_bitcast_fusion.1), channel_id=1, replica_groups=mesh['ep'=16,'tp'=2] {'ep'}, dimensions={1} | all-to-all | bytes 131072 | tf_op jit(solution)/shard_map/all_to_all | solution.py:88
  24.9 2.8 %fusion.11 = f32[256,2048]{1,0:T(8,128)} fusion(bf16[256,128]{1,0:T(8,128)(2,1)S(1)} %bitcast.59, bf16[128,512]{1,0:T(8,128)(2,1)} %param.30, bf16[128,512]{1,0:T(8,128)(2,1)} %param.29, bf16[128,512]{1,0:T(8,128)(2,1)} %param.28, bf16[128,512]{1,0:T(8,128)(2,1)} %param.27), kind=kOutput, calls=%fused_computation.18 | convolution fusion | flops 136314880 | bytes 2686976 | tf_op jit(solution)/shard_map/dot_general | solution.py:91
  27.7 0.0 reduce-scatter.2.cloned.1.call-update
  27.8 0.0 copy-start.2
  27.8 0.0 copy-start.7
  27.8 0.0 copy-done.6
  27.8 0.1 copy.42
  27.9 0.1 eq.30
  28.0 0.1 fusion.40
  28.1 0.1 reduce_window_sum.11
  28.2 0.2 select_reduce_fusion.1
  28.4 0.0 copy-start.4
  28.4 0.1 reduce_sum.93
  28.5 0.1 copy.43
  28.6 0.1 dynamic_slice.3
  28.7 0.1 multiply_cosine_fusion
  28.8 77.4 %reduce-scatter.2.cloned.1.call-done = f32[16,2048]{1,0:T(8,128)} async-done(((f32[256,2048]{1,0:T(8,128)}), f32[16,2048]{1,0:T(8,128)}) %reduce-scatter.2.cloned.1.call-update) | async-done | bytes 131088 | tf_op jit(solution)/shard_map/reduce_scatter | solution.py:90
  106.2 0.9 convert.10
  107.1 0.1 reshape.191
  107.2 0.1 reshape.193
  107.3 0.1 reshape.189
  107.4 0.1 multiply_subtract_fusion
  107.5 0.1 pad_maximum_fusion
  107.6 5.3 %fusion.62 = f32[16,8,1,64]{3,2,1,0:T(1,128)S(1)} fusion(f32[16,8,64,1]{2,3,1,0:T(1,128)S(1)} %bitcast.56, f32[16,8,64,64]{3,2,1,0:T(8,128)} %param.22), kind=kOutput, calls=%fused_computation.103 | convolution fusion | flops 6291456 | bytes 2162688 | tf_op jit(solution)/shard_map/shd,shde->she/dot_general | solution.py:46
  112.9 0.2 multiply_reduce_fusion.1
  113.1 0.1 broadcast_multiply_fusion
  113.2 0.1 reshape.183
  113.3 0.0 copy-start.1
  113.3 37.8 %all_gather.9 = bf16[256,512]{1,0:T(8,128)(2,1)S(1)} all-gather(bf16[16,512]{1,0:T(8,128)(2,1)S(1)} %fusion.46), channel_id=1, replica_groups=mesh['ep'=16,'tp'=2] {'ep'}, dimensions={0}, use_global_device_ids=true | all-gather | bytes 278528 | tf_op jit(solution)/shard_map/all_gather | solution.py:106
  151.1 0.8 convolution_convert_fusion.3
  151.9 3.5 %all-to-all-start.1 = ((bf16[16,16,128]{2,1,0:T(8,128)(2,1)}), bf16[16,16,128]{2,1,0:T(8,128)(2,1)S(1)}, u32[]{:S(2)}, u32[]{:S(2)}) async-start(bf16[16,16,128]{2,1,0:T(8,128)(2,1)} %bitcast.6), calls=%async_computation.2 | async-start | bytes 131072 | tf_op jit(solution)/shard_map/all_to_all | solution.py:110
  155.5 0.1 fusion.41
  155.6 7.4 %all-to-all-done.1 = bf16[16,16,128]{2,1,0:T(8,128)(2,1)S(1)} async-done(((bf16[16,16,128]{2,1,0:T(8,128)(2,1)}), bf16[16,16,128]{2,1,0:T(8,128)(2,1)S(1)}, u32[]{:S(2)}, u32[]{:S(2)}) %all-to-all-start.1) | async-done | bytes 65568 | tf_op jit(solution)/shard_map/all_to_all | solution.py:110
  163.0 1.9 all-gather
  164.9 0.1 fusion.23
  165.0 0.0 copy-done.2
  165.0 0.0 copy-done.7
  165.0 0.1 fusion.28
  165.1 0.1 fusion.29
  165.3 1.1 fusion.1
  166.4 3.6 %all-to-all-start.2 = ((bf16[16,8,2048]{2,1,0:T(8,128)(2,1)}), bf16[16,8,2048]{2,1,0:T(8,128)(2,1)S(1)}, u32[]{:S(2)}, u32[]{:S(2)}) async-start(bf16[16,8,2048]{2,1,0:T(8,128)(2,1)} %fusion.1), calls=%async_computation.3 | async-start | bytes 1048576 | tf_op jit(solution)/shard_map/all_to_all | solution.py:145
  170.0 0.0 all-reduce.3.cloned.1.call-start
  170.1 1.5 fusion.60
  171.6 3.0 %convolution_convert_fusion.2 = bf16[16,2048]{1,0:T(8,128)(2,1)} fusion(bf16[256,2048]{1,0:T(8,128)(2,1)} %param.39, bf16[2048,256]{1,0:T(8,128)(2,1)} %param.38, f32[16,256]{1,0:T(8,128)S(1)} %fusion.60, bf16[16,2048]{1,0:T(8,128)(2,1)S(1)} %fusion.28, f32[2048]{0:T(1024)S(1)} %copy-done.4, f32[16]{0:T(128)S(1)} %add_rsqrt_fusion.2), kind=kOutput, calls=%fused_computation.6 | convolution fusion | flops 33742848 | bytes 2252864 | tf_op jit(solution)/shard_map/dot_general | solution.py:164
  174.5 10.9 %all-to-all-done.2 = bf16[16,8,2048]{2,1,0:T(8,128)(2,1)S(1)} async-done(((bf16[16,8,2048]{2,1,0:T(8,128)(2,1)}), bf16[16,8,2048]{2,1,0:T(8,128)(2,1)S(1)}, u32[]{:S(2)}, u32[]{:S(2)}) %all-to-all-start.2) | async-done | bytes 524320 | tf_op jit(solution)/shard_map/all_to_all | solution.py:145
  185.4 1.5 fusion.9
  187.0 0.0 copy-done
  187.0 0.0 copy-done.1
  187.0 1.6 convolution_convert_fusion
  188.6 0.0 all-reduce.3.cloned.1.call-update
  188.6 17.4 %all-reduce.3.cloned.1.call-done = (bf16[16,8,2048]{2,1,0:T(8,128)(2,1)}, bf16[16,2048]{1,0:T(8,128)(2,1)}) async-done(((bf16[16,8,2048]{2,1,0:T(8,128)(2,1)}, bf16[16,2048]{1,0:T(8,128)(2,1)}), (bf16[16,8,2048]{2,1,0:T(8,128)(2,1)}, bf16[16,2048]{1,0:T(8,128)(2,1)})) %all-reduce.3.cloned.1.call-update) | async-done | bytes 589840 | tf_op jit(solution)/shard_map/psum | solution.py:154
  206.0 6.8 %all-to-all-start.3 = ((bf16[16,8,2048]{2,1,0:T(8,128)(2,1)}), bf16[16,8,2048]{2,1,0:T(8,128)(2,1)S(1)}, u32[]{:S(2)}, u32[]{:S(2)}) async-start(bf16[16,8,2048]{2,1,0:T(8,128)(2,1)} %get-tuple-element.2), calls=%async_computation.4 | async-start | bytes 1048576 | tf_op jit(solution)/shard_map/all_to_all | solution.py:155
  212.8 0.1 select_reduce_fusion
  213.0 0.0 copy-start.8
  213.0 4.3 %multiply_add_fusion = f32[16,8,64,64]{3,2,1,0:T(8,128)} fusion(f32[16,8,64,64]{3,2,1,0:T(8,128)} %param.22, f32[16,8,64]{2,1,0:T(8,128)S(1)} %reshape.193, f32[16,8,64]{2,1,0:T(8,128)S(1)} %get-tuple-element.20, f32[8]{0:T(128)S(1)} %dynamic_slice.3), kind=kLoop, calls=%fused_computation.1 | loop fusion | flops 1572864 | bytes 4259872 | tf_op jit(solution)/shard_map/add | solution.py:52
  217.3 11.1 %all-to-all-done.3 = bf16[16,8,2048]{2,1,0:T(8,128)(2,1)S(1)} async-done(((bf16[16,8,2048]{2,1,0:T(8,128)(2,1)}), bf16[16,8,2048]{2,1,0:T(8,128)(2,1)S(1)}, u32[]{:S(2)}, u32[]{:S(2)}) %all-to-all-start.3) | async-done | bytes 524320 | tf_op jit(solution)/shard_map/all_to_all | solution.py:155
  228.3 0.4 multiply_reduce_fusion
  228.8 0.7 fusion.32
  (22 shorter events, 0.1 us)
Async XLA Ops:
  7.2 179.8 %copy-start = (bf16[1,256,2048]{2,1,0:T(8,128)(2,1)S(1)}, bf16[1,256,2048]{2,1,0:T(8,128)(2,1)}, u32[]{:S(2)}) copy-start(bf16[1,256,2048]{2,1,0:T(8,128)(2,1)} %param.36) | copy-start | bytes 3145732
  7.2 20.6 %copy-start.10 = (s32[16]{0:T(128)S(1)}, s32[16]{0:T(128)}, u32[]{:S(2)}) copy-start(s32[16]{0:T(128)} %param.21) | copy-start | bytes 196
  7.2 20.6 %copy-start.6 = (s32[16,6]{0,1:T(8,128)S(1)}, s32[16,6]{0,1:T(8,128)}, u32[]{:S(2)}) copy-start(s32[16,6]{0,1:T(8,128)} %param.32) | copy-start | bytes 1156
  7.2 99.0 %reduce-scatter.2.cloned.1.call-start = ((), (), s32[]{:S(2)}) async-start(), calls=%async_computation.5 | async-start | bytes 2228224 | tf_op jit(solution)/shard_map/reduce_scatter | solution.py:90
  27.7 123.4 %copy-start.3 = (bf16[512,128]{1,0:T(8,128)(2,1)S(1)}, bf16[512,128]{1,0:T(8,128)(2,1)}, u32[]{:S(2)}) copy-start(bf16[512,128]{1,0:T(8,128)(2,1)} %param.31) | copy-start | bytes 393220
  27.8 137.2 %copy-start.2 = (bf16[16,2048]{1,0:T(8,128)(2,1)S(1)}, bf16[16,2048]{1,0:T(8,128)(2,1)}, u32[]{:S(2)}) copy-start(bf16[16,2048]{1,0:T(8,128)(2,1)} %param.20) | copy-start | bytes 196612
  27.8 137.2 %copy-start.7 = (f32[2048]{0:T(1024)S(1)}, f32[2048]{0:T(1024)}, u32[]{:S(2)}) copy-start(f32[2048]{0:T(1024)} %param.24) | copy-start | bytes 24580
  28.4 136.9 %copy-start.4 = (f32[2048]{0:T(1024)S(1)}, f32[2048]{0:T(1024)}, u32[]{:S(2)}) copy-start(f32[2048]{0:T(1024)} %param.25) | copy-start | bytes 24580
  113.3 73.7 %copy-start.1 = (bf16[1,2048,256]{2,1,0:T(8,128)(2,1)S(1)}, bf16[1,2048,256]{2,1,0:T(8,128)(2,1)}, u32[]{:S(2)}) copy-start(bf16[1,2048,256]{2,1,0:T(8,128)(2,1)} %param.35) | copy-start | bytes 3145732
  151.9 11.0 %all-to-all-start.1 = ((bf16[16,16,128]{2,1,0:T(8,128)(2,1)}), bf16[16,16,128]{2,1,0:T(8,128)(2,1)S(1)}, u32[]{:S(2)}, u32[]{:S(2)}) async-start(bf16[16,16,128]{2,1,0:T(8,128)(2,1)} %bitcast.6), calls=%async_computation.2 | async-start | bytes 131072 | tf_op jit(solution)/shard_map/all_to_all | solution.py:110
  166.4 19.0 %all-to-all-start.2 = ((bf16[16,8,2048]{2,1,0:T(8,128)(2,1)}), bf16[16,8,2048]{2,1,0:T(8,128)(2,1)S(1)}, u32[]{:S(2)}, u32[]{:S(2)}) async-start(bf16[16,8,2048]{2,1,0:T(8,128)(2,1)} %fusion.1), calls=%async_computation.3 | async-start | bytes 1048576 | tf_op jit(solution)/shard_map/all_to_all | solution.py:145
  170.0 36.0 %all-reduce.3.cloned.1.call-start = ((), (), s32[]{:S(2)}) async-start(), calls=%async_computation.6 | async-start | bytes 1179648 | tf_op jit(solution)/shard_map/psum | solution.py:154
  171.6 41.3 %copy-start.9 = (f32[16,6]{0,1:T(8,128)S(1)}, f32[16,6]{0,1:T(8,128)}, u32[]{:S(2)}) copy-start(f32[16,6]{0,1:T(8,128)} %param.33) | copy-start | bytes 1156
  206.0 22.3 %all-to-all-start.3 = ((bf16[16,8,2048]{2,1,0:T(8,128)(2,1)}), bf16[16,8,2048]{2,1,0:T(8,128)(2,1)S(1)}, u32[]{:S(2)}, u32[]{:S(2)}) async-start(bf16[16,8,2048]{2,1,0:T(8,128)(2,1)} %get-tuple-element.2), calls=%async_computation.4 | async-start | bytes 1048576 | tf_op jit(solution)/shard_map/all_to_all | solution.py:155
  212.9 15.4 %copy-start.5 = (bf16[16,2048]{1,0:T(8,128)(2,1)S(1)}, bf16[16,2048]{1,0:T(8,128)(2,1)}, u32[]{:S(2)}) copy-start(bf16[16,2048]{1,0:T(8,128)(2,1)} %get-tuple-element.3) | copy-start | bytes 196612
  213.0 15.8 %copy-start.8 = (f32[2048]{0:T(1024)S(1)}, f32[2048]{0:T(1024)}, u32[]{:S(2)}) copy-start(f32[2048]{0:T(1024)} %param.26) | copy-start | bytes 24580
Sparse Core Ops, SparseCore 0:
  27.9 78.2 reduce-scatter.1
  188.7 17.2 all-reduce.2
